TPU v7x, 32 devices: a whole 2x2x4 slice. The times are simulated.
32 devices in a mesh: ep: 8 (over z, core), tp: 4 (over y, x).
Axes of the slice: x: 2, y: 2, z: 4, core: 2. Of those that a mesh axis runs over, the one named last changes fastest.
Arguments:
- receptance: bfloat16 [2048, 2048], P('ep', 'tp'), may hold values from -6 to 6
- key_tensor: bfloat16 [2048, 2048], P('ep', 'tp'), may hold values from -6 to 6
- value_tensor: bfloat16 [2048, 2048], P('ep', 'tp'), may hold values from -6 to 6
- decay_data_input: bfloat16 [2048, 2048], P('ep', 'tp'), may hold values from -4 to 4
- correction_rate_input: bfloat16 [2048, 2048], P('ep', 'tp'), may hold values from -16 to 6
- mixer_output_gate: bfloat16 [2048, 2048], P('ep', 'tp'), may hold values from -6 to 6
- decay_channel_offset: float32 [2048], P('tp'), may hold values from -16 to -3
- head_norm_gain: float32 [2048], P('tp'), may hold values from 0.1 to 1.9
- self_key_weight: float32 [2048], P('tp'), may hold values from -2 to 2
- mixer_output_weight: bfloat16 [2048, 2048], P('tp'), may hold values from -0.125 to 0.125
- second_batch_rows: bfloat16 [1024, 2048], P('ep'), may hold values from -6 to 6
- routed_expert_index: int32 [1024, 4], P('ep'), may hold values from 0 to 7, all different within a row; in each aligned block of 128 rows (0 to 127, 128 to 255, ...) at most 96 rows name the same one
- routing_output_weight: float32 [1024, 4], P('ep'), may hold values from 0.1 to 1
- expert_norm_gain: float32 [2048], replicated, may hold values from 0.1 to 1.9
- expert_gate_weight: bfloat16 [8, 1024, 2048], P('ep', 'tp'), may hold values from -0.125 to 0.125
- expert_up_weight: bfloat16 [8, 1024, 2048], P('ep', 'tp'), may hold values from -0.125 to 0.125
- expert_down_weight: bfloat16 [8, 1024, 2048], P('ep', None, 'tp'), may hold values from -0.1875 to 0.1875
- common_expert_gate: bfloat16 [1024, 2048], P('tp'), may hold values from -0.125 to 0.125
- common_expert_up: bfloat16 [1024, 2048], P('tp'), may hold values from -0.125 to 0.125
- common_expert_down: bfloat16 [1024, 2048], P(None, 'tp'), may hold values from -0.1875 to 0.1875
Outputs:
- token_mixer_output: bfloat16 [2048, 2048], P(('ep', 'tp'))
- expert_out: bfloat16 [1024, 2048], P('ep', 'tp')
Inputs may be any that keep to these rules, and one draw needn't show every extreme that they name: `routed_expert_index`: each row names 4 different experts. Within the rows of one index of ep no expert is named by more than 96 rows, and that bound is met in some index's rows.
All inputs are finite; a program needn't handle non-finite values.
Results may differ from a plain program's by a relative error of at most 0.017.
Values may be sent and summed in bfloat16 or wider, within the bound.
A program may use at most 128 MiB of HBM per device.

v0:
```python
import math
import jax
import jax.numpy as jnp
from jax import lax
from jax.sharding import PartitionSpec as P

HEAD_CHANNELS = 64
SPAN = 64
HIGHEST = lax.Precision.HIGHEST
PRECISION = lax.Precision.HIGH
NORM_FLOOR = 1.0


def head_view(matrix):
    return matrix.astype(jnp.float32).reshape(matrix.shape[0], -1, HEAD_CHANNELS)


def complete_head_outputs(
    state_readout,
    receptance_rows,
    key_row_block,
    value_row_block,
    head_norm_gain,
    self_key_weight,
    mixer_output_gate,
):
    mean_part = jnp.mean(state_readout, axis=-1, keepdims=True)
    spread = jnp.mean(jnp.square(state_readout - mean_part), axis=-1, keepdims=True)
    normalized_rows = (state_readout - mean_part) * lax.rsqrt(spread + NORM_FLOOR)
    sequence_length = state_readout.shape[0]
    normalized_rows = normalized_rows.reshape(sequence_length, -1) * head_norm_gain
    self_key_term = (
        jnp.sum(
            receptance_rows * key_row_block * self_key_weight.reshape(-1, HEAD_CHANNELS),
            axis=-1,
            keepdims=True,
        )
        * value_row_block
    )
    mixer_result = (
        normalized_rows + self_key_term.reshape(sequence_length, -1)
    ) * mixer_output_gate.astype(jnp.float32)
    return mixer_result.astype(jnp.bfloat16)


def product(spec, left, right):
    return jnp.einsum(spec, left, right, precision=PRECISION, preferred_element_type=jnp.float32)


def lower_inverse(strict, size):
    at = jnp.arange(size)
    row, column = (at[:, None], at[None, :])
    inverse = None
    block = 1
    while block < size:
        pair = (
            (row // (2 * block) == column // (2 * block))
            & (row // block % 2 == 1)
            & (column // block % 2 == 0)
        )
        below = jnp.where(pair, strict, 0.0)
        if inverse is None:
            inverse = jnp.eye(size, dtype=jnp.float32) - below
        else:
            inverse = inverse - product(
                "nhij,nhjk->nhik", product("nhij,nhjk->nhik", inverse, below), inverse
            )
        block *= 2
    return inverse


def mixer_part(
    receptance,
    key_tensor,
    value_tensor,
    decay_data_input,
    correction_rate_input,
    mixer_output_gate,
    decay_channel_offset,
    head_norm_gain,
    self_key_weight,
    mixer_output_weight,
):
    row_count, width = receptance.shape
    head_count = width // HEAD_CHANNELS
    span = min(SPAN, row_count)
    block_count = row_count // span
    receptance_rows = head_view(receptance)
    key_row_block = head_view(key_tensor)
    value_row_block = head_view(value_tensor)

    def by_block(matrix):
        return (
            matrix.astype(jnp.float32)
            .reshape(block_count, span, head_count, HEAD_CHANNELS)
            .transpose(0, 2, 1, 3)
        )

    step_log = -math.exp(-0.5) * jax.nn.sigmoid(
        decay_channel_offset + decay_data_input.astype(jnp.float32)
    )
    at = jnp.arange(span)
    reach = (at[:, None] >= at[None, :]).astype(jnp.float32)
    step_log = by_block(step_log)
    total_log = jnp.einsum("ts,nhsd->nhtd", reach, step_log, precision=HIGHEST)
    recept, keys, values = (by_block(receptance), by_block(key_tensor), by_block(value_tensor))
    units = keys * lax.rsqrt(jnp.sum(keys * keys, axis=-1, keepdims=True) + 1.0)
    corrections = units * jax.nn.sigmoid(by_block(correction_rate_input))
    grown = jnp.exp(-total_log)
    last_log = total_log[:, :, -1:, :]
    unit_in = units * jnp.exp(total_log - step_log)
    recept_in = recept * jnp.exp(total_log)
    tail = jnp.exp(last_log - total_log)
    scores = product(
        "nhtd,nhsd->nhts",
        jnp.concatenate([unit_in, recept_in], axis=2),
        jnp.concatenate([keys * grown, corrections * grown], axis=2),
    )
    before = at[:, None] > at[None, :]
    upto = at[:, None] >= at[None, :]
    unit_key = jnp.where(before, scores[:, :, :span, :span], 0.0)
    unit_fix = jnp.where(before, scores[:, :, :span, span:], 0.0)
    read_key = jnp.where(upto, scores[:, :, span:, :span], 0.0)
    read_fix = jnp.where(upto, scores[:, :, span:, span:], 0.0)
    inverse = lower_inverse(unit_fix, span)
    key_values = product("nhts,nhsd->nhtd", jnp.concatenate([unit_key, read_key], axis=2), values)
    solved = product(
        "nhts,nhsd->nhtd", inverse, jnp.concatenate([unit_in, key_values[:, :, :span]], axis=3)
    )
    reads = jnp.concatenate([recept_in, key_values[:, :, span:]], axis=3) - product(
        "nhts,nhsd->nhtd", read_fix, solved
    )
    eye_head = jnp.eye(HEAD_CHANNELS, dtype=jnp.float32)
    fresh = product("nhtj,nhti->nhji", keys * tail, values)
    moves = jnp.concatenate([eye_head * jnp.exp(last_log), fresh], axis=3) - product(
        "nhtj,nhti->nhji", corrections * tail, solved
    )
    whole = moves[0]
    for block in range(1, block_count):
        step = product("hij,hjk->hik", moves[block, :, :, :HEAD_CHANNELS], whole)
        whole = step + jnp.concatenate(
            [jnp.zeros_like(step[..., :HEAD_CHANNELS]), moves[block, :, :, HEAD_CHANNELS:]], axis=2
        )
    everything = lax.all_gather(whole.astype(jnp.bfloat16), "ep")
    mine = lax.axis_index("ep")
    state = jnp.zeros((head_count, HEAD_CHANNELS, HEAD_CHANNELS), jnp.float32)
    for k in range(lax.axis_size("ep") - 1):
        part = everything[k].astype(jnp.float32)
        new = product("hij,hjk->hik", part[..., :HEAD_CHANNELS], state)
        state = jnp.where(k < mine, new + part[..., HEAD_CHANNELS:], state)
    starts = [state]
    for block in range(block_count - 1):
        state = (
            product("hij,hjk->hik", moves[block, :, :, :HEAD_CHANNELS], state)
            + moves[block, :, :, HEAD_CHANNELS:]
        )
        starts.append(state)
    merged_output = reads[..., HEAD_CHANNELS:] + product(
        "nhtj,nhji->nhti", reads[..., :HEAD_CHANNELS], jnp.stack(starts)
    )
    merged_output = merged_output.transpose(0, 2, 1, 3).reshape(
        row_count, head_count, HEAD_CHANNELS
    )
    mixer_result = complete_head_outputs(
        merged_output,
        receptance_rows,
        key_row_block,
        value_row_block,
        head_norm_gain,
        self_key_weight,
        mixer_output_gate,
    )
    return lax.psum_scatter(
        jnp.dot(mixer_result, mixer_output_weight, preferred_element_type=jnp.float32).astype(
            jnp.bfloat16
        ),
        "tp",
        scatter_dimension=0,
        tiled=True,
    )


def activate(rows_in, gate_part, up_part):
    pre_gate = jnp.einsum("fd,rd->fr", gate_part, rows_in, preferred_element_type=jnp.float32)
    pre_up = jnp.einsum("fd,rd->fr", up_part, rows_in, preferred_element_type=jnp.float32)
    return (jax.nn.silu(pre_gate) * pre_up).astype(jnp.bfloat16)


def expert_entry(
    second_batch_rows,
    routed_expert_index,
    routing_output_weight,
    expert_norm_gain,
    common_expert_gate,
    common_expert_up,
):
    row_count, width = second_batch_rows.shape
    top_count = routed_expert_index.shape[1]
    peer_count = lax.axis_size("ep")
    slot_count = 3 * row_count * top_count // (2 * peer_count)
    widened = second_batch_rows.astype(jnp.float32)
    normalized_rows = (
        widened
        * lax.rsqrt(jnp.mean(widened * widened, axis=-1, keepdims=True) + NORM_FLOOR)
        * expert_norm_gain
    ).astype(jnp.bfloat16)
    flat_ids = routed_expert_index.reshape(-1)
    one_hot = (flat_ids[:, None] == jnp.arange(peer_count, dtype=jnp.int32)[None, :]).astype(
        jnp.int32
    )
    slot_rank = jnp.sum((jnp.cumsum(one_hot, axis=0) - 1) * one_hot, axis=1)
    target = flat_ids * slot_count + slot_rank
    owners = jnp.arange(row_count * top_count, dtype=jnp.int32) // top_count
    source_row = jnp.full((peer_count * slot_count,), row_count, jnp.int32).at[target].set(owners)
    padded = jnp.concatenate([normalized_rows, jnp.zeros((1, width), jnp.bfloat16)], axis=0)
    outgoing = jnp.take(padded, source_row, axis=0).reshape(peer_count, slot_count, width)
    shared_hidden = activate(normalized_rows, common_expert_gate, common_expert_up)
    piece_width = width // lax.axis_size("tp")
    own_slice = lax.dynamic_slice_in_dim(
        outgoing, lax.axis_index("tp") * piece_width, piece_width, 2
    )
    arrived = lax.all_to_all(own_slice, "ep", split_axis=0, concat_axis=0, tiled=True)
    return (arrived, shared_hidden, target)


def expert_exit(
    arrived,
    shared_hidden,
    target,
    routing_output_weight,
    expert_gate_weight,
    expert_up_weight,
    expert_down_weight,
    common_expert_down,
):
    peer_count, slot_count, piece_width = arrived.shape
    row_count, top_count = routing_output_weight.shape
    out_width = expert_down_weight.shape[2]
    flat_rows = arrived.reshape(-1, piece_width)
    pieces = lax.all_gather(flat_rows, "tp", axis=1, tiled=True)
    gate_cols = expert_gate_weight[0]
    up_cols = expert_up_weight[0]
    pre_gate = jnp.einsum("fd,rd->fr", gate_cols, pieces, preferred_element_type=jnp.float32)
    pre_up = jnp.einsum("fd,rd->fr", up_cols, pieces, preferred_element_type=jnp.float32)
    routed_hidden = (jax.nn.silu(pre_gate) * pre_up).astype(jnp.bfloat16)
    both = lax.all_gather(
        jnp.concatenate([routed_hidden, shared_hidden], axis=1), "tp", axis=0, tiled=True
    )
    pieces = (both[:, : routed_hidden.shape[1]], both[:, routed_hidden.shape[1] :])
    routed_rows = expert_down_weight[0]
    routed_sum = jnp.einsum("fr,fd->rd", pieces[0], routed_rows, preferred_element_type=jnp.float32)
    shared_out = jnp.einsum(
        "fr,fd->rd", pieces[1], common_expert_down, preferred_element_type=jnp.float32
    )
    returned = lax.all_to_all(
        routed_sum.astype(jnp.bfloat16).reshape(peer_count, slot_count, out_width),
        "ep",
        split_axis=0,
        concat_axis=0,
        tiled=True,
    )
    picked = jnp.take(returned.reshape(-1, out_width), target, axis=0).reshape(
        row_count, top_count, out_width
    )
    merged_output = (
        jnp.sum(picked.astype(jnp.float32) * routing_output_weight[:, :, None], axis=1) + shared_out
    )
    return merged_output.astype(jnp.bfloat16)


def on_device(
    receptance,
    key_tensor,
    value_tensor,
    decay_data_input,
    correction_rate_input,
    mixer_output_gate,
    decay_channel_offset,
    head_norm_gain,
    self_key_weight,
    mixer_output_weight,
    second_batch_rows,
    routed_expert_index,
    routing_output_weight,
    expert_norm_gain,
    expert_gate_weight,
    expert_up_weight,
    expert_down_weight,
    common_expert_gate,
    common_expert_up,
    common_expert_down,
):
    arrived, shared_hidden, target = expert_entry(
        second_batch_rows,
        routed_expert_index,
        routing_output_weight,
        expert_norm_gain,
        common_expert_gate,
        common_expert_up,
    )
    arrived, receptance, key_tensor, value_tensor, decay_data_input, correction_rate_input = (
        lax.optimization_barrier(
            (arrived, receptance, key_tensor, value_tensor, decay_data_input, correction_rate_input)
        )
    )
    token_mixer_output = mixer_part(
        receptance,
        key_tensor,
        value_tensor,
        decay_data_input,
        correction_rate_input,
        mixer_output_gate,
        decay_channel_offset,
        head_norm_gain,
        self_key_weight,
        mixer_output_weight,
    )
    expert_out = expert_exit(
        arrived,
        shared_hidden,
        target,
        routing_output_weight,
        expert_gate_weight,
        expert_up_weight,
        expert_down_weight,
        common_expert_down,
    )
    return (token_mixer_output, expert_out)


def solution(mesh):
    in_specs = (
        P("ep", "tp"),
        P("ep", "tp"),
        P("ep", "tp"),
        P("ep", "tp"),
        P("ep", "tp"),
        P("ep", "tp"),
        P("tp"),
        P("tp"),
        P("tp"),
        P("tp", None),
        P("ep", None),
        P("ep", None),
        P("ep", None),
        P(),
        P("ep", "tp", None),
        P("ep", "tp", None),
        P("ep", None, "tp"),
        P("tp", None),
        P("tp", None),
        P(None, "tp"),
    )
    out_specs = (P(("ep", "tp"), None), P("ep", "tp"))
    return jax.shard_map(
        on_device, mesh=mesh, in_specs=in_specs, out_specs=out_specs, check_vma=False
    )
```

profile of v0, /device:TPU:0, one launch (start us, length us, event | category | flops | bytes accessed | tf_op | source)
XLA Modules:
  0.0 244.3 jit_solution(18401035282546436214)
XLA Ops:
  10.8 2.4 %scatter_custom_fusion = s32[768]{0:T(1024)S(1)} fusion(s32[512]{0:T(512)S(1)} %bitcast.192, s32[512]{0:T(512)S(1)} %add_select_fusion, s32[]{:T(128)} %constant.328.clone.1), kind=kCustom, calls=%fused_computation.208 | custom fusion | bytes 3076 | tf_op jit(solution)/shard_map/scatter | solution.py:214
  16.7 4.3 %gather_fusion = bf16[768,2048]{1,0:T(8,128)(2,1)} fusion(bf16[129,2048]{1,0:T(8,128)(2,1)S(1)} %concatenate.33, s32[1024]{0:T(1024)S(1)} %pad_clamp_fusion.1), kind=kCustom, calls=%fused_computation | custom fusion | bytes 6294528 | tf_op jit(solution)/shard_map/jit(_take)/gather | solution.py:216
  20.9 2.3 dynamic-slice_select_fusion
  23.2 6.4 %all-to-all-start = ((bf16[8,96,512]{2,1,0:T(8,128)(2,1)}), bf16[8,96,512]{2,1,0:T(8,128)(2,1)S(1)}, u32[]{:S(2)}, u32[]{:S(2)}) async-start(bf16[8,96,512]{2,1,0:T(8,128)(2,1)} %dynamic-slice_select_fusion), calls=%async_computation | async-start | bytes 1572864 | tf_op jit(solution)/shard_map/all_to_all | solution.py:222
  30.5 20.0 %all-to-all-done = bf16[8,96,512]{2,1,0:T(8,128)(2,1)S(1)} async-done(((bf16[8,96,512]{2,1,0:T(8,128)(2,1)}), bf16[8,96,512]{2,1,0:T(8,128)(2,1)S(1)}, u32[]{:S(2)}, u32[]{:S(2)}) %all-to-all-start) | async-done | bytes 786464 | tf_op jit(solution)/shard_map/all_to_all | solution.py:222
  50.7 1.9 copy.246
  52.6 2.3 add_divide_fusion
  54.9 2.2 reshape.842
  60.5 2.2 reshape.834
  62.7 2.4 reshape.884
  65.1 2.6 %copy.248 = f32[4,64,8,64]{3,1,2,0:T(8,128)} copy(f32[4,64,8,64]{1,0,3,2:T(4,128)} %reshape.884) | data formatting | bytes 1048576 | tf_op jit(solution)/shard_map/reshape | solution.py:95
  67.7 5.0 %fusion.67 = (f32[4,8,64,64]{3,2,1,0:T(8,128)S(1)}, f32[4,8,64,64]{3,2,1,0:T(8,128)S(1)}, f32[4,8,64,64]{3,2,1,0:T(8,128)S(1)}, f32[4,8,64,64]{3,2,1,0:T(8,128)S(1)}, f32[4,8,64,64]{3,2,1,0:T(8,128)}) fusion(f32[4,64,8,64]{3,2,1,0:T(8,128)} %reshape.842, f32[4,8,64]{2,1,0:T(8,128)S(1)} %add_rsqrt_fusion.1, f32[4,64,8,64]{3,1,2,0:T(8,128)S(1)} %copy.252, ...), kind=kOutput, calls=%fused_computation.114 | convolution fusion | flops 101715968 | bytes 4726784 | tf_op jit(solution)/shard_map/ts,nhsd->nhtd/dot_general | solution.py:105
  72.7 2.3 fusion.1
  82.6 1.6 convolution_subtract_fusion
  85.9 2.1 reshape.836
  87.9 2.5 %fusion.8 = f32[4,8,128,64]{3,2,1,0:T(8,128)S(1)} fusion(f32[4,8,64,64]{3,2,1,0:T(8,128)} %get-tuple-element.19, f32[4,8,64,64]{3,2,1,0:T(8,128)} %get-tuple-element.18, bf16[4,8,64,64]{3,1,2,0:T(8,128)(2,1)} %bitcast.178), kind=kOutput, calls=%fused_computation.12 | convolution fusion | flops 100925440 | bytes 2359296 | tf_op jit(solution)/shard_map/nhts,nhsd->nhtd/dot_general | solution.py:47
  94.9 1.7 convolution_subtract_fusion.5
  99.6 1.7 convolution_bitcast_fusion.4
  101.3 2.0 fusion.31
  105.2 2.0 copy.274
  107.3 3.7 %convolution_subtract_fusion.6 = f32[4,8,64,128]{3,2,1,0:T(8,128)} fusion(f32[4,8,64,128]{3,2,1,0:T(8,128)} %copy-done.8, f32[4,8,128,128]{3,2,1,0:T(8,128)} %copy-done.1, f32[4,8,64,64]{3,2,1,0:T(8,128)} %get-tuple-element.16, f32[4,8,64,64]{3,2,1,0:T(8,128)S(1)} %copy-done.7, pred[64,64]{1,0:T(8,128)(4,1)S(1)} %iota_compare_fusion.2), kind=kOutput, calls=%fused_computation.27 | convolution fusion | flops 101318656 | bytes 4722688 | tf_op jit(solution)/shard_map/nhts,nhsd->nhtd/dot_general | solution.py:47
  111.0 9.0 %all-gather.9.cloned.1.call-done = bf16[64,64,128]{2,1,0:T(8,128)(2,1)} async-done(((bf16[8,64,128]{2,1,0:T(8,128)(2,1)}), bf16[64,64,128]{2,1,0:T(8,128)(2,1)}) %all-gather.9.cloned.1.call-update) | async-done | bytes 1048592 | tf_op jit(solution)/shard_map/all_gather | solution.py:144
  123.6 41.5 %all-gather.5.cloned.1.call-done = bf16[768,2048]{1,0:T(8,128)(2,1)} async-done(((bf16[768,512]{1,0:T(8,128)(2,1)}), bf16[768,2048]{1,0:T(8,128)(2,1)}) %all-gather.5.cloned.1.call-update) | async-done | bytes 3145744 | tf_op jit(solution)/shard_map/all_gather | solution.py:240
  165.1 3.3 %convolution_bitcast_fusion.2 = f32[256,768]{0,1:T(8,128)S(1)} fusion(bf16[768,2048]{1,0:T(8,128)(2,1)} %all-gather.5.cloned.1.call-done, bf16[1,256,2048]{2,1,0:T(8,128)(2,1)} %param.34), kind=kOutput, calls=%fused_computation.32 | convolution fusion | flops 805306368 | bytes 4980736 | tf_op jit(solution)/shard_map/fd,rd->fr/dot_general | solution.py:243
  179.6 2.1 copy.273
  183.1 3.2 %convolution_convert_fusion = bf16[256,2048]{1,0:T(8,128)(2,1)} fusion(bf16[512,2048]{1,0:T(8,128)(2,1)S(1)} %copy-done, bf16[256,512]{1,0:T(8,128)(2,1)} %param.25, f32[256,512]{1,0:T(8,128)} %copy.274, bf16[256,512]{1,0:T(8,128)(2,1)S(1)} %copy-done.17, f32[256,512]{1,0:T(8,128)} %copy.273, f32[256,512]{1,0:T(8,128)} %reshape.837, ...), kind=kOutput, calls=%fused_computation.4 | convolution fusion | flops 538574848 | bytes 5769216 | tf_op jit(solution)/shard_map/dot_general | solution.py:174
  186.4 17.0 %all-gather.7.cloned.1.call-done = bf16[1024,896]{0,1:T(8,128)(2,1)} async-done(((bf16[256,896]{0,1:T(8,128)(2,1)}), bf16[1024,896]{0,1:T(8,128)(2,1)}) %all-gather.7.cloned.1.call-update) | async-done | bytes 1835024 | tf_op jit(solution)/shard_map/all_gather | solution.py:246
  203.4 3.5 %fusion.14 = bf16[768,512]{1,0:T(8,128)(2,1)} fusion(bf16[1024,896]{0,1:T(8,128)(2,1)} %all-gather.7.cloned.1.call-done, bf16[1,1024,512]{2,1,0:T(8,128)(2,1)} %param.36), kind=kOutput, calls=%fused_computation.23 | convolution fusion | flops 805699584 | bytes 3407872 | tf_op jit(solution)/shard_map/fr,fd->rd/dot_general | solution.py:251
  207.0 4.6 %all-to-all-start.1 = ((bf16[8,96,512]{2,1,0:T(8,128)(2,1)}), bf16[8,96,512]{2,1,0:T(8,128)(2,1)S(1)}, u32[]{:S(2)}, u32[]{:S(2)}) async-start(bf16[8,96,512]{2,1,0:T(8,128)(2,1)} %bitcast.187), calls=%async_computation.2 | async-start | bytes 1572864 | tf_op jit(solution)/shard_map/all_to_all | solution.py:255
  212.0 20.5 %all-to-all-done.1 = bf16[8,96,512]{2,1,0:T(8,128)(2,1)S(1)} async-done(((bf16[8,96,512]{2,1,0:T(8,128)(2,1)}), bf16[8,96,512]{2,1,0:T(8,128)(2,1)S(1)}, u32[]{:S(2)}, u32[]{:S(2)}) %all-to-all-start.1) | async-done | bytes 786464 | tf_op jit(solution)/shard_map/all_to_all | solution.py:255
  232.5 2.0 gather_fusion.1
  235.5 2.3 fusion.29
  (163 shorter events, 46.9 us)
Async XLA Ops:
  7.2 175.9 %copy-start = (bf16[512,2048]{1,0:T(8,128)(2,1)S(1)}, bf16[512,2048]{1,0:T(8,128)(2,1)}, u32[]{:S(2)}) copy-start(bf16[512,2048]{1,0:T(8,128)(2,1)} %param.29) | copy-start | bytes 6291460
  15.8 0.8 copy-start.12
  20.9 29.6 %copy-start.18 = (bf16[256,512]{1,0:T(8,128)(2,1)S(1)}, bf16[256,512]{1,0:T(8,128)(2,1)}, u32[]{:S(2)}) copy-start(bf16[256,512]{1,0:T(8,128)(2,1)} %param.21) | copy-start | bytes 786436
  20.9 31.7 %copy-start.20 = (f32[512]{0:T(512)S(1)}, f32[512]{0:T(512)}, u32[]{:S(2)}) copy-start(f32[512]{0:T(512)} %param.26) | copy-start | bytes 6148
  23.2 27.3 %all-to-all-start = ((bf16[8,96,512]{2,1,0:T(8,128)(2,1)}), bf16[8,96,512]{2,1,0:T(8,128)(2,1)S(1)}, u32[]{:S(2)}, u32[]{:S(2)}) async-start(bf16[8,96,512]{2,1,0:T(8,128)(2,1)} %dynamic-slice_select_fusion), calls=%async_computation | async-start | bytes 1572864 | tf_op jit(solution)/shard_map/all_to_all | solution.py:222
  29.6 90.4 %all-gather.9.cloned.1.call-start = ((), (), s32[]{:S(2)}) async-start(), calls=%async_computation.6 | async-start | bytes 1179648 | tf_op jit(solution)/shard_map/all_gather | solution.py:144
  50.5 6.6 %copy-start.16 = (bf16[8,96,512]{2,1,0:T(8,128)(2,1)}, bf16[8,96,512]{2,1,0:T(8,128)(2,1)S(1)}, u32[]{:S(2)}) copy-start(bf16[8,96,512]{2,1,0:T(8,128)(2,1)S(1)} %all-to-all-done) | copy-start | bytes 2359300
  72.7 2.3 copy-start.6
  72.7 2.3 copy-start.9
  75.1 9.2 %copy-start.1 = (f32[4,8,128,128]{3,2,1,0:T(8,128)}, f32[4,8,128,128]{3,2,1,0:T(8,128)S(1)}, u32[]{:S(2)}) copy-start(f32[4,8,128,128]{3,2,1,0:T(8,128)S(1)} %fusion.1) | copy-start | bytes 6291460
  90.4 1.6 copy-start.4
  90.4 1.7 copy-start.11
  92.2 1.2 copy-start.10
  92.2 1.5 copy-start.15
  93.7 1.2 copy-start.5
  94.9 1.8 copy-start.8
  96.7 1.1 copy-start.2
  97.0 2.5 %copy-start.22 = (f32[512]{0:T(512)S(1)}, f32[512]{0:T(512)}, u32[]{:S(2)}) copy-start(f32[512]{0:T(512)} %param.28) | copy-start | bytes 6148
  97.0 2.6 %copy-start.13 = (bf16[128,2048]{1,0:T(8,128)(2,1)S(1)}, bf16[128,2048]{1,0:T(8,128)(2,1)}, u32[]{:S(2)}) copy-start(bf16[128,2048]{1,0:T(8,128)(2,1)} %copy-done.12) | copy-start | bytes 1572868
  98.7 66.4 %all-gather.5.cloned.1.call-start = ((), (), s32[]{:S(2)}) async-start(), calls=%async_computation.4 | async-start | bytes 3932160 | tf_op jit(solution)/shard_map/all_gather | solution.py:240
  99.4 104.0 %all-gather.7.cloned.1.call-start = ((), (), s32[]{:S(2)}) async-start(), calls=%async_computation.5 | async-start | bytes 2293760 | tf_op jit(solution)/shard_map/all_gather | solution.py:246
  101.3 6.0 %copy-start.7 = (f32[4,8,64,64]{3,2,1,0:T(8,128)S(1)}, f32[4,8,64,64]{3,2,1,0:T(8,128)}, u32[]{:S(2)}) copy-start(f32[4,8,64,64]{3,2,1,0:T(8,128)} %copy-done.6) | copy-start | bytes 1572868
  123.6 44.9 %copy-start.25 = (bf16[1,256,2048]{2,1,0:T(8,128)(2,1)S(1)}, bf16[1,256,2048]{2,1,0:T(8,128)(2,1)}, u32[]{:S(2)}) copy-start(bf16[1,256,2048]{2,1,0:T(8,128)(2,1)} %param.35) | copy-start | bytes 3145732
  165.1 3.4 %copy-start.24 = (bf16[768,2048]{1,0:T(8,128)(2,1)S(1)}, bf16[768,2048]{1,0:T(8,128)(2,1)}, u32[]{:S(2)}) copy-start(bf16[768,2048]{1,0:T(8,128)(2,1)} %all-gather.5.cloned.1.call-done) | copy-start | bytes 9437188
  169.5 6.1 %copy-start.3 = (f32[4,8,64,128]{3,2,1,0:T(8,128)S(1)}, f32[4,8,64,128]{3,2,1,0:T(8,128)}, u32[]{:S(2)}) copy-start(f32[4,8,64,128]{3,2,1,0:T(8,128)} %copy-done.2) | copy-start | bytes 3145732
  170.4 67.4 %reduce-scatter.2.cloned.1.call-start = ((), (), s32[]{:S(2)}) async-start(), calls=%async_computation.3 | async-start | bytes 1310720 | tf_op jit(solution)/shard_map/reduce_scatter | solution.py:173
  171.9 4.5 %copy-start.14 = (f32[4,8,64,128]{3,2,1,0:T(8,128)S(1)}, f32[4,8,64,128]{3,2,1,0:T(8,128)}, u32[]{:S(2)}) copy-start(f32[4,8,64,128]{3,2,1,0:T(8,128)} %convolution_subtract_fusion.6) | copy-start | bytes 3145732
  179.6 3.5 %copy-start.17 = (bf16[256,512]{1,0:T(8,128)(2,1)S(1)}, bf16[256,512]{1,0:T(8,128)(2,1)}, u32[]{:S(2)}) copy-start(bf16[256,512]{1,0:T(8,128)(2,1)} %param.22) | copy-start | bytes 786436
  179.6 3.5 %copy-start.21 = (f32[512]{0:T(512)S(1)}, f32[512]{0:T(512)}, u32[]{:S(2)}) copy-start(f32[512]{0:T(512)} %param.27) | copy-start | bytes 6148
  186.4 25.3 %copy-start.23 = (f32[128,4]{0,1:T(4,128)S(1)}, f32[128,4]{0,1:T(4,128)}, u32[]{:S(2)}) copy-start(f32[128,4]{0,1:T(4,128)} %param.32) | copy-start | bytes 6148
  186.4 25.5 %copy-start.19 = (s32[128,4]{0,1:T(4,128)S(1)}, s32[128,4]{0,1:T(4,128)}, u32[]{:S(2)}) copy-start(s32[128,4]{0,1:T(4,128)} %param.31) | copy-start | bytes 6148
  207.0 25.6 %all-to-all-start.1 = ((bf16[8,96,512]{2,1,0:T(8,128)(2,1)}), bf16[8,96,512]{2,1,0:T(8,128)(2,1)S(1)}, u32[]{:S(2)}, u32[]{:S(2)}) async-start(bf16[8,96,512]{2,1,0:T(8,128)(2,1)} %bitcast.187), calls=%async_computation.2 | async-start | bytes 1572864 | tf_op jit(solution)/shard_map/all_to_all | solution.py:255
Sparse Core Ops, SparseCore 0:
  98.8 21.1 all-gather.8
  121.8 43.2 all-gather.4
  170.5 32.8 all-gather.6
  206.7 27.9 reduce-scatter.1
where the time goes:
time: 246 us; the launch traced here: 244 us
  waiting for transfers between devices  109 us (44%)
  matrix products  54.7 us (22%)
  local copies, waits for them, and re-layouts  38.5 us (16%)
  other arithmetic  16.2 us (7%)
  between operations  14.6 us (6%)
  starting transfers between devices  11.6 us (5%)
    all_gather x1, waiting for transfers between devices, expert_exit(): pieces = lax.all_gather(flat_rows, 'tp', axis=1, tiled=True)  41.5 us
    dot_general x30, matrix products, product(): jnp.einsum(spec, left, right, precision=PRECISION, preferred_element_type...  32.6 us
    all_to_all x1, waiting for transfers between devices, expert_exit(): lax.all_to_all(routed_sum.astype(jnp.bfloat16).reshape(peer_count, slot_c...  20.5 us
    all_to_all x1, waiting for transfers between devices, expert_entry(): lax.all_to_all(own_slice, 'ep', split_axis=0, concat_axis=0, tiled=True)  20 us
    all_gather x1, waiting for transfers between devices, expert_exit(): lax.all_gather(jnp.concatenate([routed_hidden, shared_hidden], axis=1), '...  17 us
    reshape x6, local copies, waits for them, and re-layouts, by_block(): return matrix.astype(jnp.float32).reshape(block_count, span, head_count,...  12.3 us
    all_gather x1, waiting for transfers between devices, mixer_part(): everything = lax.all_gather(whole.astype(jnp.bfloat16), 'ep')  9.03 us
    all_to_all x1, starting transfers between devices, expert_entry(): lax.all_to_all(own_slice, 'ep', split_axis=0, concat_axis=0, tiled=True)  6.35 us
  transfers between devices with their start and end apart: 6, of which 5 were waited for; matrix products, arithmetic and copies ran while one was open for 17% of the time, Pallas kernels for 0%

commit v1 on v0

--- a/solution.py
+++ b/solution.py
@@ -237,7 +237,12 @@
     row_count, top_count = routing_output_weight.shape
     out_width = expert_down_weight.shape[2]
     flat_rows = arrived.reshape(-1, piece_width)
-    pieces = lax.all_gather(flat_rows, "tp", axis=1, tiled=True)
+    ring = [flat_rows]
+    for hop in range(3):
+        ring.append(lax.ppermute(ring[-1], "tp", [(dev, (dev + 1) % 4) for dev in range(4)]))
+    pieces = jnp.roll(
+        jnp.concatenate(ring[::-1], axis=1), (lax.axis_index("tp") + 1) * ring[0].shape[1], axis=1
+    )
     gate_cols = expert_gate_weight[0]
     up_cols = expert_up_weight[0]
     pre_gate = jnp.einsum("fd,rd->fr", gate_cols, pieces, preferred_element_type=jnp.float32)

time: 246 us -> 241 us (0.980)
  waiting for transfers between devices: 109 us -> 98.1 us
  local copies, waits for them, and re-layouts: 38.5 us -> 43.7 us
  matrix products: 54.7 us -> 51.7 us
    all_gather x1 -> x0, waiting for transfers between devices: 41.5 us -> none  [expert_exit(): pieces = lax.all_gather(flat_rows, 'tp', axis=1, tiled=True)]
    ppermute x0 -> x3, waiting for transfers between devices: none -> 41.1 us  [expert_exit(): lax.ppermute(ring[-1], 'tp', [(dev, (dev + 1) % 4) for dev in range(4)])]
    all_gather x1, waiting for transfers between devices: 9.03 us -> 0.01 us  [mixer_part(): everything = lax.all_gather(whole.astype(jnp.bfloat16), 'ep')]
    unnamed x54 -> x73, local copies, waits for them, and re-layouts: 3.55 us -> 12.1 us
  transfers between devices with their start and end apart: 6 -> 8, of which waited for: 5 -> 6; matrix products, arithmetic and copies ran while one was open for 17% -> 17% of each run, Pallas kernels for 0% -> 0%
where the time goes in v1:
time: 241 us; the launch traced here: 240 us
  waiting for transfers between devices  98.1 us (41%)
  matrix products  51.7 us (21%)
  local copies, waits for them, and re-layouts  43.7 us (18%)
  between operations  16.4 us (7%)
  other arithmetic  16.2 us (7%)
  starting transfers between devices  13.6 us (6%)
    ppermute x3, waiting for transfers between devices, expert_exit(): lax.ppermute(ring[-1], 'tp', [(dev, (dev + 1) % 4) for dev in range(4)])  41.1 us
    dot_general x30, matrix products, product(): jnp.einsum(spec, left, right, precision=PRECISION, preferred_element_type...  32 us
    all_to_all x1, waiting for transfers between devices, expert_exit(): lax.all_to_all(routed_sum.astype(jnp.bfloat16).reshape(peer_count, slot_c...  20.5 us
    all_to_all x1, waiting for transfers between devices, expert_entry(): lax.all_to_all(own_slice, 'ep', split_axis=0, concat_axis=0, tiled=True)  20 us
    all_gather x1, waiting for transfers between devices, expert_exit(): lax.all_gather(jnp.concatenate([routed_hidden, shared_hidden], axis=1), '...  16.4 us
    unnamed x73, local copies, waits for them, and re-layouts  12.1 us
    reshape x6, local copies, waits for them, and re-layouts, by_block(): return matrix.astype(jnp.float32).reshape(block_count, span, head_count,...  10.3 us
    all_to_all x1, starting transfers between devices, expert_entry(): lax.all_to_all(own_slice, 'ep', split_axis=0, concat_axis=0, tiled=True)  6.35 us
  transfers between devices with their start and end apart: 8, of which 6 were waited for; matrix products, arithmetic and copies ran while one was open for 17% of the time, Pallas kernels for 0%

profile of v1, /device:TPU:0, one launch (start us, length us, event | category | flops | bytes accessed | tf_op | source)
XLA Modules:
  0.0 239.7 jit_solution(8954415010661315971)
XLA Ops:
  11.6 2.4 %scatter_custom_fusion = s32[768]{0:T(1024)S(1)} fusion(s32[512]{0:T(512)S(1)} %bitcast.192, s32[512]{0:T(512)S(1)} %add_select_fusion, s32[]{:T(128)} %constant.346.clone.1), kind=kCustom, calls=%fused_computation.219 | custom fusion | bytes 3076 | tf_op jit(solution)/shard_map/scatter | solution.py:214
  17.5 4.3 %gather_fusion = bf16[768,2048]{1,0:T(8,128)(2,1)} fusion(bf16[129,2048]{1,0:T(8,128)(2,1)S(1)} %concatenate.39, s32[1024]{0:T(1024)S(1)} %pad_clamp_fusion.1), kind=kCustom, calls=%fused_computation | custom fusion | bytes 6294528 | tf_op jit(solution)/shard_map/jit(_take)/gather | solution.py:216
  21.8 2.3 dynamic-slice_select_fusion
  24.1 6.4 %all-to-all-start = ((bf16[8,96,512]{2,1,0:T(8,128)(2,1)}), bf16[8,96,512]{2,1,0:T(8,128)(2,1)S(1)}, u32[]{:S(2)}, u32[]{:S(2)}) async-start(bf16[8,96,512]{2,1,0:T(8,128)(2,1)} %dynamic-slice_select_fusion), calls=%async_computation | async-start | bytes 1572864 | tf_op jit(solution)/shard_map/all_to_all | solution.py:222
  31.4 20.0 %all-to-all-done = bf16[8,96,512]{2,1,0:T(8,128)(2,1)S(1)} async-done(((bf16[8,96,512]{2,1,0:T(8,128)(2,1)}), bf16[8,96,512]{2,1,0:T(8,128)(2,1)S(1)}, u32[]{:S(2)}, u32[]{:S(2)}) %all-to-all-start) | async-done | bytes 786464 | tf_op jit(solution)/shard_map/all_to_all | solution.py:222
  52.9 2.4 %add_divide_fusion = (f32[256,512]{1,0:T(8,128)}, f32[256,512]{1,0:T(8,128)}) fusion(bf16[256,512]{1,0:T(8,128)(2,1)} %param.24, bf16[256,512]{1,0:T(8,128)(2,1)} %param.23, f32[512]{0:T(512)S(1)} %copy-done.26), kind=kLoop, calls=%fused_computation.137 | loop fusion | flops 1310720 | bytes 1574912 | tf_op jit(solution)/shard_map/div | solution.py:108
  55.3 2.2 reshape.842
  57.5 1.4 reshape.885
  59.0 1.6 copy.252
  60.9 2.2 reshape.834
  64.6 2.6 %copy.248 = f32[4,64,8,64]{3,1,2,0:T(8,128)} copy(f32[4,64,8,64]{1,0,3,2:T(4,128)} %reshape.884) | data formatting | bytes 1048576 | tf_op jit(solution)/shard_map/reshape | solution.py:95
  67.2 5.0 %fusion.75 = (f32[4,8,64,64]{3,2,1,0:T(8,128)S(1)}, f32[4,8,64,64]{3,2,1,0:T(8,128)S(1)}, f32[4,8,64,64]{3,2,1,0:T(8,128)S(1)}, f32[4,8,64,64]{3,2,1,0:T(8,128)S(1)}, f32[4,8,64,64]{3,2,1,0:T(8,128)}) fusion(f32[4,64,8,64]{3,2,1,0:T(8,128)} %reshape.842, f32[4,8,64]{2,1,0:T(8,128)S(1)} %add_rsqrt_fusion.1, f32[4,64,8,64]{3,1,2,0:T(8,128)S(1)} %copy.252, ...), kind=kOutput, calls=%fused_computation.116 | convolution fusion | flops 101715968 | bytes 4726784 | tf_op jit(solution)/shard_map/ts,nhsd->nhtd/dot_general | solution.py:105
  72.1 2.3 fusion.5
  82.0 1.6 convolution_subtract_fusion
  83.6 1.7 slice_select_fusion.4
  86.4 2.5 %fusion.12 = f32[4,8,128,64]{3,2,1,0:T(8,128)S(1)} fusion(f32[4,8,64,64]{3,2,1,0:T(8,128)} %get-tuple-element.19, f32[4,8,64,64]{3,2,1,0:T(8,128)} %get-tuple-element.18, bf16[4,8,64,64]{3,1,2,0:T(8,128)(2,1)} %bitcast.179), kind=kOutput, calls=%fused_computation.16 | convolution fusion | flops 100925440 | bytes 2359296 | tf_op jit(solution)/shard_map/nhts,nhsd->nhtd/dot_general | solution.py:47
  93.3 1.7 convolution_subtract_fusion.5
  96.6 1.5 collective-permute-start
  99.5 1.9 convolution_bitcast_fusion.2
  101.4 15.2 %collective-permute-done = bf16[768,512]{1,0:T(8,128)(2,1)} collective-permute-done((bf16[768,512]{1,0:T(8,128)(2,1)S(1)}, bf16[768,512]{1,0:T(8,128)(2,1)}, u32[]{:S(2)}, u32[]{:S(2)}) %collective-permute-start) | collective-permute-done | bytes 786464 | tf_op jit(solution)/shard_map/ppermute | solution.py:242
  117.2 1.7 fusion.39
  120.1 3.2 %convolution_subtract_fusion.6 = f32[4,8,64,128]{3,2,1,0:T(8,128)} fusion(f32[4,8,64,128]{3,2,1,0:T(8,128)S(1)} %copy-done.10, f32[4,8,128,128]{3,2,1,0:T(8,128)S(1)} %copy-done.2, f32[4,8,64,64]{3,2,1,0:T(8,128)} %get-tuple-element.16, f32[4,8,64,64]{3,2,1,0:T(8,128)S(1)} %copy-done.8, pred[64,64]{1,0:T(8,128)(4,1)S(1)} %iota_compare_fusion.2), kind=kOutput, calls=%fused_computation.31 | convolution fusion | flops 101318656 | bytes 4726784 | tf_op jit(solution)/shard_map/nhts,nhsd->nhtd/dot_general | solution.py:47
  123.2 12.7 %collective-permute-done.1 = bf16[768,512]{1,0:T(8,128)(2,1)} collective-permute-done((bf16[768,512]{1,0:T(8,128)(2,1)}, bf16[768,512]{1,0:T(8,128)(2,1)}, u32[]{:S(2)}, u32[]{:S(2)}) %collective-permute-start.1) | collective-permute-done | bytes 786464 | tf_op jit(solution)/shard_map/ppermute | solution.py:242
  141.4 13.1 %collective-permute-done.2 = bf16[768,512]{1,0:T(8,128)(2,1)} collective-permute-done((bf16[768,512]{1,0:T(8,128)(2,1)}, bf16[768,512]{1,0:T(8,128)(2,1)}, u32[]{:S(2)}, u32[]{:S(2)}) %collective-permute-start.2) | collective-permute-done | bytes 786464 | tf_op jit(solution)/shard_map/ppermute | solution.py:242
  174.7 2.1 copy.273
  178.2 3.2 %convolution_convert_fusion = bf16[256,2048]{1,0:T(8,128)(2,1)} fusion(bf16[512,2048]{1,0:T(8,128)(2,1)S(1)} %copy-done, bf16[256,512]{1,0:T(8,128)(2,1)} %param.25, f32[256,512]{1,0:T(8,128)} %copy.274, bf16[256,512]{1,0:T(8,128)(2,1)S(1)} %copy-done.23, f32[256,512]{1,0:T(8,128)} %copy.273, f32[256,512]{1,0:T(8,128)} %reshape.837, ...), kind=kOutput, calls=%fused_computation.8 | convolution fusion | flops 538574848 | bytes 5769216 | tf_op jit(solution)/shard_map/dot_general | solution.py:174
  181.4 16.4 %all-gather.4.cloned.1.call-done = bf16[1024,896]{0,1:T(8,128)(2,1)} async-done(((bf16[256,896]{0,1:T(8,128)(2,1)}), bf16[1024,896]{0,1:T(8,128)(2,1)}) %all-gather.4.cloned.1.call-update) | async-done | bytes 1835024 | tf_op jit(solution)/shard_map/all_gather | solution.py:251
  197.9 3.6 %fusion.18 = bf16[768,512]{1,0:T(8,128)(2,1)} fusion(bf16[1024,896]{0,1:T(8,128)(2,1)} %all-gather.4.cloned.1.call-done, bf16[1,1024,512]{2,1,0:T(8,128)(2,1)} %param.36), kind=kOutput, calls=%fused_computation.27 | convolution fusion | flops 805699584 | bytes 3407872 | tf_op jit(solution)/shard_map/fr,fd->rd/dot_general | solution.py:256
  201.4 4.6 %all-to-all-start.1 = ((bf16[8,96,512]{2,1,0:T(8,128)(2,1)}), bf16[8,96,512]{2,1,0:T(8,128)(2,1)S(1)}, u32[]{:S(2)}, u32[]{:S(2)}) async-start(bf16[8,96,512]{2,1,0:T(8,128)(2,1)} %bitcast.187), calls=%async_computation.2 | async-start | bytes 1572864 | tf_op jit(solution)/shard_map/all_to_all | solution.py:260
  206.5 20.5 %all-to-all-done.1 = bf16[8,96,512]{2,1,0:T(8,128)(2,1)S(1)} async-done(((bf16[8,96,512]{2,1,0:T(8,128)(2,1)}), bf16[8,96,512]{2,1,0:T(8,128)(2,1)S(1)}, u32[]{:S(2)}, u32[]{:S(2)}) %all-to-all-start.1) | async-done | bytes 786464 | tf_op jit(solution)/shard_map/all_to_all | solution.py:260
  227.0 2.0 gather_fusion.1
  230.0 2.3 fusion.37
  (183 shorter events, 56.6 us)
Async XLA Ops:
  8.0 170.2 %copy-start = (bf16[512,2048]{1,0:T(8,128)(2,1)S(1)}, bf16[512,2048]{1,0:T(8,128)(2,1)}, u32[]{:S(2)}) copy-start(bf16[512,2048]{1,0:T(8,128)(2,1)} %param.29) | copy-start | bytes 6291460
  21.8 29.6 %copy-start.24 = (bf16[256,512]{1,0:T(8,128)(2,1)S(1)}, bf16[256,512]{1,0:T(8,128)(2,1)}, u32[]{:S(2)}) copy-start(bf16[256,512]{1,0:T(8,128)(2,1)} %param.21) | copy-start | bytes 786436
  21.8 31.1 %copy-start.26 = (f32[512]{0:T(512)S(1)}, f32[512]{0:T(512)}, u32[]{:S(2)}) copy-start(f32[512]{0:T(512)} %param.26) | copy-start | bytes 6148
  24.1 27.3 %all-to-all-start = ((bf16[8,96,512]{2,1,0:T(8,128)(2,1)}), bf16[8,96,512]{2,1,0:T(8,128)(2,1)S(1)}, u32[]{:S(2)}, u32[]{:S(2)}) async-start(bf16[8,96,512]{2,1,0:T(8,128)(2,1)} %dynamic-slice_select_fusion), calls=%async_computation | async-start | bytes 1572864 | tf_op jit(solution)/shard_map/all_to_all | solution.py:222
  30.4 107.3 %all-gather.6.cloned.1.call-start = ((), (), s32[]{:S(2)}) async-start(), calls=%async_computation.5 | async-start | bytes 1179648 | tf_op jit(solution)/shard_map/all_gather | solution.py:144
  51.4 6.1 %copy-start.13 = (bf16[8,96,512]{2,1,0:T(8,128)(2,1)}, bf16[8,96,512]{2,1,0:T(8,128)(2,1)S(1)}, u32[]{:S(2)}) copy-start(bf16[8,96,512]{2,1,0:T(8,128)(2,1)S(1)} %all-to-all-done) | copy-start | bytes 2359300
  51.5 6.0 %copy-start.20 = (bf16[256,512]{0,1:T(8,128)(2,1)}, bf16[256,512]{0,1:T(8,128)(2,1)S(1)}, u32[]{:S(2)}) copy-start(bf16[256,512]{0,1:T(8,128)(2,1)S(1)} %copy.250) | copy-start | bytes 786436
  52.9 10.3 %copy-start.21 = (bf16[256,512]{0,1:T(8,128)(2,1)}, bf16[256,512]{0,1:T(8,128)(2,1)S(1)}, u32[]{:S(2)}) copy-start(bf16[256,512]{0,1:T(8,128)(2,1)S(1)} %copy.246) | copy-start | bytes 786436
  72.1 2.3 copy-start.7
  72.1 2.3 copy-start.11
  74.5 9.2 %copy-start.1 = (f32[4,8,128,128]{3,2,1,0:T(8,128)}, f32[4,8,128,128]{3,2,1,0:T(8,128)S(1)}, u32[]{:S(2)}) copy-start(f32[4,8,128,128]{3,2,1,0:T(8,128)S(1)} %fusion.5) | copy-start | bytes 6291460
  88.9 1.7 copy-start.15
  93.3 1.8 copy-start.9
  95.1 3.3 %copy-start.3 = (f32[4,8,64,128]{3,2,1,0:T(8,128)}, f32[4,8,64,128]{3,2,1,0:T(8,128)S(1)}, u32[]{:S(2)}) copy-start(f32[4,8,64,128]{3,2,1,0:T(8,128)S(1)} %convolution_subtract_fusion.5) | copy-start | bytes 3145732
  95.1 4.3 %copy-start.28 = (f32[512]{0:T(512)S(1)}, f32[512]{0:T(512)}, u32[]{:S(2)}) copy-start(f32[512]{0:T(512)} %param.28) | copy-start | bytes 6148
  95.1 4.4 %copy-start.17 = (bf16[128,2048]{1,0:T(8,128)(2,1)S(1)}, bf16[128,2048]{1,0:T(8,128)(2,1)}, u32[]{:S(2)}) copy-start(bf16[128,2048]{1,0:T(8,128)(2,1)} %copy-done.16) | copy-start | bytes 1572868
  96.6 20.0 %collective-permute-start = (bf16[768,512]{1,0:T(8,128)(2,1)S(1)}, bf16[768,512]{1,0:T(8,128)(2,1)}, u32[]{:S(2)}, u32[]{:S(2)}) collective-permute-start(bf16[768,512]{1,0:T(8,128)(2,1)S(1)} %bitcast.175), channel_id=1, source_target_pairs={{0,1},{1,2},{2,3},{3,0},{4,5},{5,6},{6,7},{7,4},{8,9},{9,10},{10,1... | collective-permute-start | bytes 2359304 | tf_op jit(solution)/shard_map/ppermute | solution.py:242
  99.3 98.5 %all-gather.4.cloned.1.call-start = ((), (), s32[]{:S(2)}) async-start(), calls=%async_computation.4 | async-start | bytes 2293760 | tf_op jit(solution)/shard_map/all_gather | solution.py:251
  99.5 20.5 %copy-start.2 = (f32[4,8,128,128]{3,2,1,0:T(8,128)S(1)}, f32[4,8,128,128]{3,2,1,0:T(8,128)}, u32[]{:S(2)}) copy-start(f32[4,8,128,128]{3,2,1,0:T(8,128)} %copy-done.1) | copy-start | bytes 6291460
  99.5 20.6 %copy-start.8 = (f32[4,8,64,64]{3,2,1,0:T(8,128)S(1)}, f32[4,8,64,64]{3,2,1,0:T(8,128)}, u32[]{:S(2)}) copy-start(f32[4,8,64,64]{3,2,1,0:T(8,128)} %copy-done.7) | copy-start | bytes 1572868
  99.5 20.6 %copy-start.10 = (f32[4,8,64,128]{3,2,1,0:T(8,128)S(1)}, f32[4,8,64,128]{3,2,1,0:T(8,128)}, u32[]{:S(2)}) copy-start(f32[4,8,64,128]{3,2,1,0:T(8,128)} %copy-done.9) | copy-start | bytes 3145732
  116.6 19.3 %collective-permute-start.1 = (bf16[768,512]{1,0:T(8,128)(2,1)}, bf16[768,512]{1,0:T(8,128)(2,1)}, u32[]{:S(2)}, u32[]{:S(2)}) collective-permute-start(bf16[768,512]{1,0:T(8,128)(2,1)} %collective-permute-done), channel_id=1, source_target_pairs={{0,1},{1,2},{2,3},{3,0},{4,5},{5,6},{6,7},{7,4},{8,9},{9,10},{10,1... | collective-permute-start | bytes 2359304 | tf_op jit(solution)/shard_map/ppermute | solution.py:242
  136.0 18.5 %collective-permute-start.2 = (bf16[768,512]{1,0:T(8,128)(2,1)}, bf16[768,512]{1,0:T(8,128)(2,1)}, u32[]{:S(2)}, u32[]{:S(2)}) collective-permute-start(bf16[768,512]{1,0:T(8,128)(2,1)} %collective-permute-done.1), channel_id=1, source_target_pairs={{0,1},{1,2},{2,3},{3,0},{4,5},{5,6},{6,7},{7,4},{8,9},{9,10},{10,1... | collective-permute-start | bytes 2359304 | tf_op jit(solution)/shard_map/ppermute | solution.py:242
  159.6 2.7 %copy-start.30 = (bf16[1,256,2048]{2,1,0:T(8,128)(2,1)S(1)}, bf16[1,256,2048]{2,1,0:T(8,128)(2,1)}, u32[]{:S(2)}) copy-start(bf16[1,256,2048]{2,1,0:T(8,128)(2,1)} %param.34) | copy-start | bytes 3145732
  164.6 6.1 %copy-start.4 = (f32[4,8,64,128]{3,2,1,0:T(8,128)S(1)}, f32[4,8,64,128]{3,2,1,0:T(8,128)}, u32[]{:S(2)}) copy-start(f32[4,8,64,128]{3,2,1,0:T(8,128)} %copy-done.3) | copy-start | bytes 3145732
  165.4 66.8 %reduce-scatter.2.cloned.1.call-start = ((), (), s32[]{:S(2)}) async-start(), calls=%async_computation.3 | async-start | bytes 1310720 | tf_op jit(solution)/shard_map/reduce_scatter | solution.py:173
  166.9 4.5 %copy-start.18 = (f32[4,8,64,128]{3,2,1,0:T(8,128)S(1)}, f32[4,8,64,128]{3,2,1,0:T(8,128)}, u32[]{:S(2)}) copy-start(f32[4,8,64,128]{3,2,1,0:T(8,128)} %convolution_subtract_fusion.6) | copy-start | bytes 3145732
  174.7 3.5 %copy-start.23 = (bf16[256,512]{1,0:T(8,128)(2,1)S(1)}, bf16[256,512]{1,0:T(8,128)(2,1)}, u32[]{:S(2)}) copy-start(bf16[256,512]{1,0:T(8,128)(2,1)} %param.22) | copy-start | bytes 786436
  174.7 3.5 %copy-start.27 = (f32[512]{0:T(512)S(1)}, f32[512]{0:T(512)}, u32[]{:S(2)}) copy-start(f32[512]{0:T(512)} %param.27) | copy-start | bytes 6148
  181.4 24.8 %copy-start.29 = (f32[128,4]{0,1:T(4,128)S(1)}, f32[128,4]{0,1:T(4,128)}, u32[]{:S(2)}) copy-start(f32[128,4]{0,1:T(4,128)} %param.32) | copy-start | bytes 6148
  181.4 24.9 %copy-start.25 = (s32[128,4]{0,1:T(4,128)S(1)}, s32[128,4]{0,1:T(4,128)}, u32[]{:S(2)}) copy-start(s32[128,4]{0,1:T(4,128)} %param.31) | copy-start | bytes 6148
  201.4 25.6 %all-to-all-start.1 = ((bf16[8,96,512]{2,1,0:T(8,128)(2,1)}), bf16[8,96,512]{2,1,0:T(8,128)(2,1)S(1)}, u32[]{:S(2)}, u32[]{:S(2)}) async-start(bf16[8,96,512]{2,1,0:T(8,128)(2,1)} %bitcast.187), calls=%async_computation.2 | async-start | bytes 1572864 | tf_op jit(solution)/shard_map/all_to_all | solution.py:260
  (8 other events, 10.8 us)
Sparse Core Ops, SparseCore 0:
  99.5 19.8 all-gather.5
Sparse Core Ops, SparseCore 1:
  165.5 32.3 all-gather.3
  201.2 27.8 reduce-scatter.1
